TPU v7x, 32 devices: a whole 2x2x4 slice. The times are simulated.
32 devices in a mesh: tp: 8 (over z, y), dp: 4 (over x, core).
Axes of the slice: x: 2, y: 2, z: 4, core: 2. Of those that a mesh axis runs over, the one named last changes fastest.
Arguments:
- stream: bfloat16 [128, 4096], P(None, ('dp', 'tp')), may hold values from -16 to 16
- lengths: int32 [128], P('dp'), may hold values from 1 to 64, 1024 in all
- prior_state: float32 [2, 128, 4096], P(None, 'dp', 'tp'), may hold values from -6 to 6
- prior_window: bfloat16 [2, 128, 3, 4096], P(None, 'dp', None, 'tp'), may hold values from -6 to 6
- norm_gain: float32 [2, 4096], P(None, 'dp'), may hold values from 0.1 to 1.9
- w_branch: bfloat16 [2, 4096, 4096], P(None, 'dp', 'tp'), may hold values from -0.09375 to 0.09375
- w_gate_branch: bfloat16 [2, 4096, 4096], P(None, 'dp', 'tp'), may hold values from -0.09375 to 0.09375
- conv_taps: bfloat16 [2, 4, 4096], P(None, None, 'tp'), may hold values from -3 to 3
- w_in_gate: bfloat16 [2, 256, 4096], P(None, None, 'tp'), may hold values from -0.375 to 0.375
- w_rec_gate: bfloat16 [2, 256, 4096], P(None, None, 'tp'), may hold values from -0.375 to 0.375
- decay_param: float32 [2, 4096], P(None, 'tp'), may hold values from -1 to 4
- w_out: bfloat16 [2, 4096, 4096], P(None, 'tp', 'dp'), may hold values from -0.1875 to 0.1875
Outputs:
- mixed_out: bfloat16 [128, 4096], P(None, ('dp', 'tp'))
- new_state: float32 [2, 128, 4096], P(None, 'dp', 'tp')
- new_window: bfloat16 [2, 128, 3, 4096], P(None, 'dp', None, 'tp')
All inputs are finite; a program needn't handle non-finite values. No bound on the sum of `lengths` on one device may be relied on, other than what follows from the above.
Results may differ from a plain program's by a relative error of at most 0.014.
Values may be sent and summed in bfloat16 or wider, within the bound.
A program may use at most 64 MiB of HBM per device.

v0:
```python
import jax
import jax.numpy as jnp
from jax import lax
from jax.sharding import PartitionSpec as P

D = 4096
BLOCK = 256


epsilon = 1e-06


def from_partner(block, axis, apart):
    count = lax.axis_size(axis)
    route = []
    for low in range(count):
        high = low | 1 << apart
        if high != low and high < count:
            route += [(low, high), (high, low)]
    return lax.ppermute(block, axis, route)


def norm_rows(block_rows, gain_values, squares):
    scaling = lax.rsqrt(squares / D + epsilon)
    return (block_rows.astype(jnp.float32) * scaling * gain_values).astype(jnp.bfloat16)


def normed_input(stream_local, gain_block):
    own_width = stream_local.shape[1]
    offset = lax.axis_index("tp") * own_width
    widened = stream_local.astype(jnp.float32)
    squares = lax.psum(jnp.sum(widened * widened, axis=1, keepdims=True), ("tp", "dp"))
    own_gain = lax.dynamic_slice_in_dim(gain_block, offset, own_width, 0)
    result = lax.all_gather(norm_rows(stream_local, own_gain, squares), "tp", axis=1, tiled=True)
    return result


def peer_block(convolved):
    col_count = convolved.shape[1]
    group_size = max(BLOCK // col_count, 1)
    device = lax.axis_index("tp")
    grouped = convolved
    for bit_number in range(group_size.bit_length() - 1):
        partner = from_partner(grouped, "tp", bit_number)
        is_upper = device // (1 << bit_number) % 2 == 1
        grouped = jnp.where(
            is_upper,
            jnp.concatenate([partner, grouped], axis=1),
            jnp.concatenate([grouped, partner], axis=1),
        )
    return grouped


def block_gates(grouped, weight):
    row_count = grouped.shape[0]
    col_count = weight.shape[1]
    blocks = max(col_count // BLOCK, 1)
    block_cols = min(col_count, BLOCK)
    inputs = grouped.reshape(row_count, blocks, BLOCK)
    tables = weight.reshape(BLOCK, blocks, block_cols)
    mapped = jnp.einsum("rnk,knc->rnc", inputs, tables, preferred_element_type=jnp.float32)
    return mapped.reshape(row_count, col_count)


def recurrent_step(
    normed,
    lengths,
    prior_state,
    prior_window,
    w_branch,
    w_gate_branch,
    conv_taps,
    w_in_gate,
    w_rec_gate,
    decay_param,
    w_out,
    stream_local,
):
    col_count = w_branch.shape[1]
    summed = lax.psum_scatter(
        jnp.concatenate(
            [
                jnp.dot(normed, w_branch, preferred_element_type=jnp.float32),
                jnp.dot(normed, w_gate_branch, preferred_element_type=jnp.float32),
            ],
            axis=1,
        ).astype(jnp.bfloat16),
        "dp",
        scatter_dimension=0,
        tiled=True,
    ).astype(jnp.float32)
    branch = summed[:, :col_count].astype(jnp.bfloat16)
    gate_in = summed[:, col_count:].astype(jnp.bfloat16)
    depth = prior_window.shape[1]
    needed = depth + 1 - jnp.arange(depth, dtype=jnp.int32)
    living = lengths[:, None, None] >= needed[None, :, None]
    history = jnp.where(living, prior_window, jnp.zeros_like(prior_window))
    window = jnp.concatenate([history, branch[:, None, :]], axis=1)
    convolved = jnp.sum(
        window.astype(jnp.float32) * conv_taps.astype(jnp.float32)[None], axis=1
    ).astype(jnp.bfloat16)
    grouped = peer_block(convolved)
    input_gate = jax.nn.sigmoid(block_gates(grouped, w_in_gate))
    recur_gate = jax.nn.sigmoid(block_gates(grouped, w_rec_gate))
    log_keep = 8.0 * recur_gate * jax.nn.log_sigmoid(decay_param)
    keeping = jnp.exp(log_keep)
    feeding = jnp.sqrt(-jnp.expm1(2.0 * log_keep))
    earlier = jnp.where(lengths[:, None] >= 2, prior_state, jnp.zeros_like(prior_state))
    state = keeping * earlier + feeding * input_gate * convolved.astype(jnp.float32)
    readout = (state * jax.nn.gelu(gate_in.astype(jnp.float32))).astype(jnp.bfloat16)
    mixed = jnp.dot(
        lax.all_gather(readout, "dp", axis=0, tiled=True), w_out, preferred_element_type=jnp.float32
    )
    own_width = stream_local.shape[1]
    offset = lax.axis_index("tp") * own_width
    own_cols = lax.dynamic_slice_in_dim(mixed, offset, own_width, 1) + stream_local.astype(
        jnp.float32
    )
    terms = lax.dynamic_update_slice_in_dim(mixed, own_cols, offset, 1)
    return (terms, state, window[:, 1:])


def body(
    stream,
    lengths,
    prior_state,
    prior_window,
    norm_gain,
    w_branch,
    w_gate_branch,
    conv_taps,
    w_in_gate,
    w_rec_gate,
    decay_param,
    w_out,
):
    normed = normed_input(stream, norm_gain[0])
    terms, state_first, window_first = recurrent_step(
        normed,
        lengths,
        prior_state[0],
        prior_window[0],
        w_branch[0],
        w_gate_branch[0],
        conv_taps[0],
        w_in_gate[0],
        w_rec_gate[0],
        decay_param[0],
        w_out[0],
        stream,
    )
    carried = lax.psum(terms, "tp").astype(jnp.bfloat16)
    widened = carried.astype(jnp.float32)
    squares = lax.psum(jnp.sum(widened * widened, axis=1, keepdims=True), "dp")
    normed = norm_rows(carried, norm_gain[1], squares)
    own_width = stream.shape[1]
    first = lax.dynamic_slice_in_dim(carried, lax.axis_index("tp") * own_width, own_width, 1)
    terms, state_second, window_second = recurrent_step(
        normed,
        lengths,
        prior_state[1],
        prior_window[1],
        w_branch[1],
        w_gate_branch[1],
        conv_taps[1],
        w_in_gate[1],
        w_rec_gate[1],
        decay_param[1],
        w_out[1],
        first,
    )
    second = lax.psum_scatter(terms, "tp", scatter_dimension=1, tiled=True).astype(jnp.bfloat16)
    return (
        second,
        jnp.stack([state_first, state_second]),
        jnp.stack([window_first, window_second]),
    )


def solution(mesh):
    placed = (
        P(None, ("dp", "tp")),
        P("dp"),
        P(None, "dp", "tp"),
        P(None, "dp", None, "tp"),
        P(None, "dp"),
        P(None, "dp", "tp"),
        P(None, "dp", "tp"),
        P(None, None, "tp"),
        P(None, None, "tp"),
        P(None, None, "tp"),
        P(None, "tp"),
        P(None, "tp", "dp"),
    )
    return jax.shard_map(
        body,
        mesh=mesh,
        in_specs=placed,
        out_specs=(P(None, ("dp", "tp")), P(None, "dp", "tp"), P(None, "dp", None, "tp")),
        check_vma=False,
    )
```

profile of v0, /device:TPU:0, one launch (start us, length us, event | category | flops | bytes accessed | tf_op | source)
XLA Modules:
  0.0 261.5 jit_solution(7721415944423887952)
XLA Ops:
  7.2 0.0 reduce-scatter.4.cloned.1.call-start
  7.2 0.9 fusion.45
  8.1 42.0 %psum.21 = f32[128,1]{0,1:T(1,128)S(1)} all-reduce(f32[128,1]{0,1:T(1,128)S(1)} %bitcast.133), channel_id=1, replica_groups=mesh['tp'=8,'dp'=4] {'tp','dp'}, use_global_device_ids=true, to_apply=%region_1.0 | all-reduce | flops 128 | bytes 1024 | tf_op jit(solution)/shard_map/psum | solution.py:32
  50.1 1.4 fusion.76
  51.5 0.8 fusion.47
  52.3 26.4 %all_gather.9 = bf16[128,1024]{1,0:T(8,128)(2,1)S(1)} all-gather(bf16[128,128]{1,0:T(8,128)(2,1)S(1)} %fusion.47), channel_id=1, replica_groups=mesh['tp'=8,'dp'=4] {'tp'}, dimensions={1}, use_global_device_ids=true | all-gather | bytes 294912 | tf_op jit(solution)/shard_map/all_gather | solution.py:34
  78.7 1.6 convolution_convert_fusion.2
  80.3 0.0 copy-start.20
  80.4 1.5 convolution_convert_fusion.3
  81.9 0.7 pad_maximum_fusion
  82.6 0.0 reduce-scatter.4.cloned.1.call-update
  82.7 0.0 reduce-scatter.6.cloned.1.call-start
  82.8 0.0 copy-start.5
  82.8 0.0 copy-start.1
  82.8 1.2 fusion.74
  84.1 0.1 broadcast_compare_fusion
  84.2 0.5 broadcast_compare_fusion.1
  84.7 0.8 copy.52
  85.5 0.1 copy.51
  85.7 0.0 copy-start.8
  85.7 1.0 bitcast_select_fusion.1
  86.8 14.5 %reduce-scatter.4.cloned.1.call-done = bf16[32,1024]{1,0:T(8,128)(2,1)} async-done(((bf16[128,1024]{1,0:T(8,128)(2,1)}), bf16[32,1024]{1,0:T(8,128)(2,1)}) %reduce-scatter.4.cloned.1.call-update) | async-done | bytes 65552 | tf_op jit(solution)/shard_map/reduce_scatter | solution.py:80
  101.3 0.8 slice_bitcast_fusion.1
  102.1 0.0 copy-start.9
  102.1 1.2 fusion.8
  103.3 0.6 copy-done.12
  103.9 0.2 fusion.11
  104.2 0.9 fusion.37
  105.0 5.4 %all_gather.10 = bf16[128,512]{1,0:T(8,128)(2,1)S(1)} all-gather(bf16[32,512]{1,0:T(8,128)(2,1)S(1)} %fusion.37), channel_id=1, replica_groups=mesh['tp'=8,'dp'=4] {'dp'}, dimensions={0}, use_global_device_ids=true | all-gather | bytes 163840 | tf_op jit(solution)/shard_map/all_gather | solution.py:112
  110.4 0.3 fusion.16
  110.8 43.3 %all-reduce.1 = bf16[128,1024]{1,0:T(8,128)(2,1)S(1)} all-reduce(f32[128,1024]{1,0:T(8,128)S(1)} %fusion.48), channel_id=1, replica_groups=mesh['tp'=8,'dp'=4] {'tp'}, use_global_device_ids=true, to_apply=%region_4.5 | all-reduce | flops 131072 | bytes 786432 | tf_op jit(solution)/shard_map/psum | solution.py:152
  154.1 0.1 fusion.26
  154.2 5.9 %psum.23 = f32[128,1]{0,1:T(1,128)S(1)} all-reduce(f32[128,1]{0,1:T(1,128)S(1)} %bitcast.134), channel_id=1, replica_groups=mesh['tp'=8,'dp'=4] {'dp'}, use_global_device_ids=true, to_apply=%region_6.7 | all-reduce | flops 128 | bytes 1024 | tf_op jit(solution)/shard_map/psum | solution.py:154
  160.2 1.6 convolution_convert_fusion
  161.8 1.6 convolution_convert_fusion.1
  163.4 0.7 pad_maximum_fusion.1
  164.1 0.0 reduce-scatter.6.cloned.1.call-update
  164.1 0.0 reduce-scatter.8.cloned.1.call-start
  164.2 0.1 copy.54
  164.3 0.1 copy.53
  164.5 16.2 %reduce-scatter.6.cloned.1.call-done = bf16[32,1024]{1,0:T(8,128)(2,1)} async-done(((bf16[128,1024]{1,0:T(8,128)(2,1)}), bf16[32,1024]{1,0:T(8,128)(2,1)}) %reduce-scatter.6.cloned.1.call-update) | async-done | bytes 65552 | tf_op jit(solution)/shard_map/reduce_scatter | solution.py:80
  180.7 0.8 slice_bitcast_fusion
  181.5 0.2 fusion.2
  181.7 0.2 fusion.5
  182.0 0.6 copy-done.13
  182.5 0.9 fusion.42
  183.4 0.0 copy-start.7
  183.4 5.5 %all_gather.11 = bf16[128,512]{1,0:T(8,128)(2,1)S(1)} all-gather(bf16[32,512]{1,0:T(8,128)(2,1)S(1)} %fusion.42), channel_id=1, replica_groups=mesh['tp'=8,'dp'=4] {'dp'}, dimensions={0}, use_global_device_ids=true | all-gather | bytes 163840 | tf_op jit(solution)/shard_map/all_gather | solution.py:112
  189.0 0.3 fusion.12
  189.4 0.8 copy-done
  190.1 0.0 reduce-scatter.8.cloned.1.call-update
  190.2 0.9 copy.34
  191.1 0.1 div.87
  191.1 0.9 copy.30
  192.0 0.1 div.86
  192.1 0.9 copy.42
  193.0 0.1 div.89
  193.1 0.1 copy.38
  193.1 0.1 div.88
  193.2 0.1 fusion.39
  193.4 0.7 pad_maximum_fusion.5
  194.0 0.7 pad_maximum_fusion.2
  194.7 58.8 %reduce-scatter.8.cloned.1.call-done = f32[128,128]{1,0:T(8,128)} async-done(((f32[128,1024]{1,0:T(8,128)}), f32[128,128]{1,0:T(8,128)}) %reduce-scatter.8.cloned.1.call-update) | async-done | bytes 65552 | tf_op jit(solution)/shard_map/reduce_scatter | solution.py:172
  253.5 1.5 convert_element_type.132
  (50 shorter events, 0.3 us)
Async XLA Ops:
  7.2 94.1 %reduce-scatter.4.cloned.1.call-start = ((), (), s32[]{:S(2)}) async-start(), calls=%async_computation.3 | async-start | bytes 327680 | tf_op jit(solution)/shard_map/reduce_scatter | solution.py:80
  78.7 4.0 %copy-start.19 = (f32[2,512]{1,0:T(2,128)S(1)}, f32[2,512]{1,0:T(2,128)}, u32[]{:S(2)}) copy-start(f32[2,512]{1,0:T(2,128)} %param.22) | copy-start | bytes 12292
  78.7 4.0 %copy-start.4 = (bf16[2,256,512]{2,1,0:T(8,128)(2,1)S(1)}, bf16[2,256,512]{2,1,0:T(8,128)(2,1)}, u32[]{:S(2)}) copy-start(bf16[2,256,512]{2,1,0:T(8,128)(2,1)} %param.20) | copy-start | bytes 1572868
  80.3 3.7 %copy-start.20 = (s32[32]{0:T(128)S(1)}, s32[32]{0:T(128)}, u32[]{:S(2)}) copy-start(s32[32]{0:T(128)} %param.13) | copy-start | bytes 388
  82.6 3.0 %copy-start.16 = (bf16[2,4,512]{2,1,0:T(4,128)(2,1)S(1)}, bf16[2,4,512]{2,1,0:T(4,128)(2,1)}, u32[]{:S(2)}) copy-start(bf16[2,4,512]{2,1,0:T(4,128)(2,1)} %param.19) | copy-start | bytes 24580
  82.7 98.0 %reduce-scatter.6.cloned.1.call-start = ((), (), s32[]{:S(2)}) async-start(), calls=%async_computation.4 | async-start | bytes 327680 | tf_op jit(solution)/shard_map/reduce_scatter | solution.py:80
  82.8 21.3 %copy-start.5 = (f32[2,32,512]{2,1,0:T(8,128)S(1)}, f32[2,32,512]{2,1,0:T(8,128)}, u32[]{:S(2)}) copy-start(f32[2,32,512]{2,1,0:T(8,128)} %param.14) | copy-start | bytes 393220
  82.8 27.6 %copy-start.1 = (bf16[2,512,1024]{2,1,0:T(8,128)(2,1)S(1)}, bf16[2,512,1024]{2,1,0:T(8,128)(2,1)}, u32[]{:S(2)}) copy-start(bf16[2,512,1024]{2,1,0:T(8,128)(2,1)} %param.23) | copy-start | bytes 6291460
  85.7 25.1 %copy-start.8 = (bf16[128,128]{1,0:T(8,128)(2,1)S(1)}, bf16[128,128]{1,0:T(8,128)(2,1)}, u32[]{:S(2)}) copy-start(bf16[128,128]{1,0:T(8,128)(2,1)} %param.12) | copy-start | bytes 98308
  86.8 24.0 %copy-start.2 = (bf16[32,3,512]{2,0,1:T(8,128)(2,1)}, bf16[32,3,512]{2,0,1:T(8,128)(2,1)S(1)}, u32[]{:S(2)}) copy-start(bf16[32,3,512]{2,0,1:T(8,128)(2,1)S(1)} %get-tuple-element.8) | copy-start | bytes 294916
  102.1 2.1 copy-start.9
  103.3 0.6 copy-start.12
  104.1 0.9 copy-start.11
  163.4 19.2 %copy-start.6 = (f32[2,32,512]{2,1,0:T(8,128)S(1)}, f32[2,32,512]{2,1,0:T(8,128)}, u32[]{:S(2)}) copy-start(f32[2,32,512]{2,1,0:T(8,128)} %param.14) | copy-start | bytes 393220
  163.4 19.1 %copy-start.17 = (pred[32]{0:T(512)(128)(4,1)S(1)}, pred[32]{0:T(512)(128)(4,1)}, u32[]{:S(2)}) copy-start(pred[32]{0:T(512)(128)(4,1)} %broadcast_compare_fusion.1) | copy-start | bytes 100
  164.1 89.4 %reduce-scatter.8.cloned.1.call-start = ((), (), s32[]{:S(2)}) async-start(), calls=%async_computation.5 | async-start | bytes 589824 | tf_op jit(solution)/shard_map/reduce_scatter | solution.py:172
  181.7 1.7 copy-start.15
  181.7 10.4 %copy-start.3 = (bf16[32,3,512]{2,0,1:T(8,128)(2,1)S(1)}, bf16[32,3,512]{2,0,1:T(8,128)(2,1)}, u32[]{:S(2)}) copy-start(bf16[32,3,512]{2,0,1:T(8,128)(2,1)} %copy-done.2) | copy-start | bytes 294916
  181.9 0.6 copy-start.13
  183.4 9.7 %copy-start.14 = (f32[2,32,256]{2,1,0:T(8,128)S(1)}, f32[2,32,256]{2,1,0:T(8,128)}, u32[]{:S(2)}) copy-start(f32[2,32,256]{2,1,0:T(8,128)} %copy-done.13) | copy-start | bytes 196612
  183.4 9.8 %copy-start.7 = (f32[2,32,512]{2,1,0:T(8,128)S(1)}, f32[2,32,512]{2,1,0:T(8,128)}, u32[]{:S(2)}) copy-start(f32[2,32,512]{2,1,0:T(8,128)} %param.14) | copy-start | bytes 393220
  183.4 9.8 %copy-start.10 = (bf16[32,512]{1,0:T(8,128)(2,1)S(1)}, bf16[32,512]{1,0:T(8,128)(2,1)}, u32[]{:S(2)}) copy-start(bf16[32,512]{1,0:T(8,128)(2,1)} %copy-done.9) | copy-start | bytes 98308
  183.4 9.8 %copy-start.18 = (pred[32]{0:T(512)(128)(4,1)S(1)}, pred[32]{0:T(512)(128)(4,1)}, u32[]{:S(2)}) copy-start(pred[32]{0:T(512)(128)(4,1)} %broadcast_compare_fusion.1) | copy-start | bytes 100
  189.3 0.8 copy-start
Sparse Core Ops, SparseCore 0:
  82.8 18.4 reduce-scatter.3
  164.3 16.3 reduce-scatter.5
  190.3 63.2 reduce-scatter.7
where the time goes:
time: 263 us; the launch traced here: 262 us
  blocking collectives  129 us (49%)
  waiting for transfers between devices  89.6 us (34%)
  between operations  14.3 us (5%)
  local copies, waits for them, and re-layouts  10.4 us (4%)
  other arithmetic  9.79 us (4%)
  matrix products  8.71 us (3%)
    reduce_scatter x1, waiting for transfers between devices, body(): lax.psum_scatter(terms, 'tp', scatter_dimension=1, tiled=True)  58.8 us
    psum x1, blocking collectives, body(): carried = lax.psum(terms, 'tp').astype(jnp.bfloat16)  43.3 us
    psum x1, blocking collectives, normed_input(): lax.psum(jnp.sum(widened * widened, axis=1, keepdims=True), ('tp', 'dp'))  42 us
    reduce_scatter x2, waiting for transfers between devices, recurrent_step(): lax.psum_scatter(jnp.concatenate([jnp.dot(normed, w_branch, preferred_ele...  30.7 us
    all_gather x1, blocking collectives, normed_input(): lax.all_gather(norm_rows(stream_local, own_gain, squares), 'tp', axis=1,...  26.4 us
    all_gather x2, blocking collectives, recurrent_step(): lax.all_gather(readout, 'dp', axis=0, tiled=True)  11 us
    psum x1, blocking collectives, body(): squares = lax.psum(jnp.sum(widened * widened, axis=1, keepdims=True), 'dp')  5.93 us
  transfers between devices with their start and end apart: 3, of which 3 were waited for; matrix products, arithmetic and copies ran while one was open for 3% of the time, Pallas kernels for 0%

commit v1 on v0

--- a/solution.py
+++ b/solution.py
@@ -1,6 +1,10 @@
+import functools
+
 import jax
 import jax.numpy as jnp
 from jax import lax
+from jax.experimental import pallas as pl
+from jax.experimental.pallas import tpu as pltpu
 from jax.sharding import PartitionSpec as P
 
 D = 4096
@@ -177,6 +181,389 @@
     )
 
 
+HALVES = 2
+MESH = pl.DeviceIdType.MESH
+
+
+def negative_expm1(z):
+    series = -z * (1.0 + z / 2.0 * (1.0 + z / 3.0 * (1.0 + z / 4.0 * (1.0 + z / 5.0))))
+    return jnp.where(z > -0.1, series, 1.0 - jnp.exp(z))
+
+
+def fused_kernel(
+    nt,
+    nd,
+    halves,
+    stream,
+    lengths,
+    prior_state,
+    prior_window,
+    norm_gain,
+    w_branch,
+    w_gate_branch,
+    conv_taps,
+    w_in_gate,
+    w_rec_gate,
+    decay_param,
+    w_out,
+    mixed_out,
+    new_state,
+    new_window,
+    xg,
+    part,
+    pr,
+    ro,
+    rg,
+    mx,
+    ms,
+    len_v,
+    state_v,
+    win_v,
+    gain_v,
+    wp_v,
+    taps_v,
+    gates_v,
+    decay_v,
+    wo_v,
+    state_o,
+    win_o,
+    mix_o,
+    in_sem,
+    out_sem,
+    xs,
+    xr,
+    ps,
+    prs,
+    gs,
+    gr,
+    ms_s,
+    ms_r,
+):
+    t = lax.axis_index("tp")
+    d = lax.axis_index("dp")
+    layers = w_branch.shape[0]
+    rows, own = stream.shape[1], stream.shape[2]
+    r = rows // halves
+    cols = w_branch.shape[2]
+    width = w_branch.shape[1]
+
+    barrier = pltpu.get_barrier_semaphore()
+    tp_peers = [lax.rem(t + k, nt) for k in range(1, nt)]
+    dp_peers = [lax.rem(d + k, nd) for k in range(1, nd)]
+    for peer in tp_peers:
+        pl.semaphore_signal(barrier, inc=1, device_id={"tp": peer}, device_id_type=MESH)
+    for peer in dp_peers:
+        pl.semaphore_signal(barrier, inc=1, device_id={"dp": peer}, device_id_type=MESH)
+
+    counter = [0]
+
+    def load(src, dst):
+        copy = pltpu.make_async_copy(src, dst, in_sem.at[counter[0]])
+        counter[0] += 1
+        copy.start()
+        return copy
+
+    c_stream = load(stream, xg.at[0, t])
+    c_gain = load(norm_gain, gain_v)
+    c_len = load(lengths, len_v)
+    loads = []
+    for l in range(layers):
+        c_w = [load(w_branch.at[l], wp_v.at[l, 0]), load(w_gate_branch.at[l], wp_v.at[l, 1])]
+        c_s = [
+            load(prior_window.at[l], win_v.at[l]),
+            load(prior_state.at[l], state_v.at[l]),
+            load(w_in_gate.at[l], gates_v.at[l, 0]),
+            load(w_rec_gate.at[l], gates_v.at[l, 1]),
+        ]
+        if l == 0:
+            c_s += [load(conv_taps, taps_v), load(decay_param, decay_v), c_len]
+        c_o = [load(w_out.at[l], wo_v.at[l])]
+        loads.append((c_w, c_s, c_o))
+
+    sends = []
+
+    def send(src, dst, ssem, rsem, axis, peer):
+        copy = pltpu.make_async_remote_copy(
+            src_ref=src,
+            dst_ref=dst,
+            send_sem=ssem,
+            recv_sem=rsem,
+            device_id={axis: peer},
+            device_id_type=MESH,
+        )
+        copy.start()
+        sends.append(copy)
+
+    def arrived(dst, ssem, rsem, axis, peer):
+        pltpu.make_async_remote_copy(
+            src_ref=dst,
+            dst_ref=dst,
+            send_sem=ssem,
+            recv_sem=rsem,
+            device_id={axis: peer},
+            device_id_type=MESH,
+        ).wait_recv()
+
+    def cut(h):
+        return slice(h * r, (h + 1) * r)
+
+    def send_features(l, h):
+        for k, peer in enumerate(tp_peers):
+            block = xg.at[l, t, :, pl.ds(h * r, r), :]
+            send(block, block, xs.at[l, h, k], xr.at[l, h, t], "tp", peer)
+
+    def project(l, h):
+        for k, peer in enumerate(tp_peers):
+            block = xg.at[l, peer, :, pl.ds(h * r, r), :]
+            arrived(block, xs.at[l, h, k], xr.at[l, h, peer], "tp", peer)
+        if h == 0:
+            if l == 0:
+                c_gain.wait()
+            for copy in loads[l][0]:
+                copy.wait()
+        squares = jnp.zeros((nd * r, own), jnp.float32)
+        pieces = []
+        for j in range(nt):
+            x = xg[l, j, :, cut(h), :].reshape(nd * r, own).astype(jnp.float32)
+            squares = squares + x * x
+            gain = gain_v[l : l + 1, j * own : (j + 1) * own]
+            pieces.append((x * gain).astype(jnp.bfloat16))
+        normed = jnp.concatenate(pieces, axis=1)
+        total = jnp.sum(squares, axis=1, keepdims=True)
+        high = total.astype(jnp.bfloat16).astype(jnp.float32)
+        lane = lax.broadcasted_iota(jnp.int32, (nd * r, 128), 1)
+        both = jnp.where(lane < 64, high, total - high).astype(jnp.bfloat16)
+        part[l, h, :, :, 2 * cols :] = both.reshape(nd, r, 128)
+        for w in range(2):
+            product = jnp.dot(normed, wp_v[l, w], preferred_element_type=jnp.float32)
+            part[l, h, :, :, w * cols : (w + 1) * cols] = product.astype(jnp.bfloat16).reshape(
+                nd, r, cols
+            )
+        for k, peer in enumerate(dp_peers):
+            send(
+                part.at[l, h, peer],
+                pr.at[l, h, d],
+                ps.at[l, h, k],
+                prs.at[l, h, d],
+                "dp",
+                peer,
+            )
+
+    def recur(l, h):
+        summed = part[l, h, d].astype(jnp.float32)
+        if h == 0:
+            for copy in loads[l][1]:
+                copy.wait()
+        length = jnp.sum(
+            jnp.where(
+                lax.broadcasted_iota(jnp.int32, (r, rows), 0) + h * r
+                == lax.broadcasted_iota(jnp.int32, (r, rows), 1),
+                jnp.broadcast_to(len_v[...].astype(jnp.float32), (r, rows)),
+                0.0,
+            ),
+            axis=1,
+            keepdims=True,
+        )
+        depth = prior_window.shape[1]
+        history = []
+        for m in range(depth):
+            row = win_v[l, m, cut(h), :].astype(jnp.float32)
+            history.append(jnp.where(length >= depth + 1 - m, row, 0.0))
+        taps = taps_v[l].astype(jnp.float32)
+        before = history[0] * taps[0:1]
+        for m in range(1, depth):
+            before = before + history[m] * taps[m : m + 1]
+        raw = decay_v[l : l + 1]
+        log_decay = jnp.minimum(raw, 0.0) - jnp.log1p(jnp.exp(-jnp.abs(raw)))
+        earlier = jnp.where(length >= 2, state_v[l, cut(h), :], 0.0)
+
+        for k, peer in enumerate(dp_peers):
+            arrived(pr.at[l, h, peer], ps.at[l, h, k], prs.at[l, h, peer], "dp", peer)
+        for peer in dp_peers:
+            summed = summed + pr[l, h, peer].astype(jnp.float32)
+        squares = summed[:, 2 * cols : 2 * cols + 1] + summed[:, 2 * cols + 64 : 2 * cols + 65]
+        scaling = lax.rsqrt(squares / (width * nd) + epsilon)
+        branch = (summed[:, :cols] * scaling).astype(jnp.bfloat16)
+        gate_in = (summed[:, cols : 2 * cols] * scaling).astype(jnp.bfloat16)
+        for m in range(1, depth):
+            win_o[l, m - 1, cut(h), :] = history[m].astype(jnp.bfloat16)
+        win_o[l, depth - 1, cut(h), :] = branch
+        convolved = (before + branch.astype(jnp.float32) * taps[depth : depth + 1]).astype(
+            jnp.bfloat16
+        )
+        mapped = []
+        for w in range(2):
+            mapped.append(
+                jnp.concatenate(
+                    [
+                        jnp.dot(
+                            convolved[:, n * BLOCK : (n + 1) * BLOCK],
+                            gates_v[l, w, :, n * BLOCK : (n + 1) * BLOCK],
+                            preferred_element_type=jnp.float32,
+                        )
+                        for n in range(cols // BLOCK)
+                    ],
+                    axis=1,
+                )
+            )
+        input_gate = jax.nn.sigmoid(mapped[0])
+        recur_gate = jax.nn.sigmoid(mapped[1])
+        log_keep = 8.0 * recur_gate * log_decay
+        feeding = jnp.sqrt(negative_expm1(2.0 * log_keep))
+        state = jnp.exp(log_keep) * earlier + feeding * input_gate * convolved.astype(jnp.float32)
+        state_o[l, cut(h), :] = state
+        ro[l, h] = (state * jax.nn.gelu(gate_in.astype(jnp.float32))).astype(jnp.bfloat16)
+        for k, peer in enumerate(dp_peers):
+            send(ro.at[l, h], rg.at[l, h, d], gs.at[l, h, k], gr.at[l, h, d], "dp", peer)
+        rg[l, h, d] = ro[l, h]
+
+    def mix(l, h):
+        if h == 0:
+            for copy in loads[l][2]:
+                copy.wait()
+        for k, peer in enumerate(dp_peers):
+            arrived(rg.at[l, h, peer], gs.at[l, h, k], gr.at[l, h, peer], "dp", peer)
+        readout = rg[l, h].reshape(nd * r, cols)
+        mixed = jnp.dot(readout, wo_v[l], preferred_element_type=jnp.float32)
+        for j in range(nt):
+            mx[l, h, j] = mixed[:, j * own : (j + 1) * own].astype(jnp.bfloat16)
+        for k, peer in enumerate(tp_peers):
+            send(mx.at[l, h, peer], ms.at[l, h, t], ms_s.at[l, h, k], ms_r.at[l, h, t], "tp", peer)
+
+    def collect(l, h):
+        total = mx[l, h, t].astype(jnp.float32)
+        total = total + xg[l, t, :, cut(h), :].reshape(nd * r, own).astype(jnp.float32)
+        for k, peer in enumerate(tp_peers):
+            arrived(ms.at[l, h, peer], ms_s.at[l, h, k], ms_r.at[l, h, peer], "tp", peer)
+            total = total + ms[l, h, peer].astype(jnp.float32)
+        result = total.astype(jnp.bfloat16).reshape(nd, r, own)
+        if l + 1 < layers:
+            xg[l + 1, t, :, cut(h), :] = result
+            send_features(l + 1, h)
+        else:
+            mix_o[:, cut(h), :] = result
+
+    stores = []
+
+    def store(src, dst):
+        copy = pltpu.make_async_copy(src, dst, out_sem.at[len(stores)])
+        copy.start()
+        stores.append(copy)
+
+    c_stream.wait()
+    pl.semaphore_wait(barrier, nt - 1 + nd - 1)
+    for h in range(halves):
+        send_features(0, h)
+    for l in range(layers):
+        for h in range(halves):
+            project(l, h)
+        for h in range(halves):
+            recur(l, h)
+        for h in range(halves):
+            mix(l, h)
+        store(state_o.at[l], new_state.at[l])
+        store(win_o.at[l], new_window.at[l])
+        for h in range(halves):
+            collect(l, h)
+    store(mix_o, mixed_out)
+    for copy in sends:
+        copy.wait_send()
+    for copy in stores:
+        copy.wait()
+
+
+def fused(
+    nt,
+    nd,
+    halves,
+    stream,
+    lengths,
+    prior_state,
+    prior_window,
+    norm_gain,
+    w_branch,
+    w_gate_branch,
+    conv_taps,
+    w_in_gate,
+    w_rec_gate,
+    decay_param,
+    w_out,
+):
+    layers, width, cols = w_branch.shape
+    batch, own = stream.shape
+    rows = batch // nd
+    r = rows // halves
+    depth = prior_window.shape[2]
+    window = prior_window.transpose(0, 2, 1, 3)
+    bf16, f32 = jnp.bfloat16, jnp.float32
+    anywhere = pl.BlockSpec(memory_space=pl.ANY)
+    dma = pltpu.SemaphoreType.DMA
+    mixed, state, new_window = pl.pallas_call(
+        functools.partial(fused_kernel, nt, nd, halves),
+        out_shape=(
+            jax.ShapeDtypeStruct((nd, rows, own), bf16),
+            jax.ShapeDtypeStruct(prior_state.shape, f32),
+            jax.ShapeDtypeStruct(window.shape, bf16),
+        ),
+        in_specs=[anywhere] * 12,
+        out_specs=(anywhere,) * 3,
+        scratch_shapes=[
+            pltpu.VMEM((layers, nt, nd, rows, own), bf16),
+            pltpu.VMEM((layers, halves, nd, r, 2 * cols + 128), bf16),
+            pltpu.VMEM((layers, halves, nd, r, 2 * cols + 128), bf16),
+            pltpu.VMEM((layers, halves, r, cols), bf16),
+            pltpu.VMEM((layers, halves, nd, r, cols), bf16),
+            pltpu.VMEM((layers, halves, nt, nd * r, own), bf16),
+            pltpu.VMEM((layers, halves, nt, nd * r, own), bf16),
+            pltpu.VMEM((1, rows), jnp.int32),
+            pltpu.VMEM(prior_state.shape, f32),
+            pltpu.VMEM(window.shape, bf16),
+            pltpu.VMEM(norm_gain.shape, f32),
+            pltpu.VMEM((layers, 2, width, cols), bf16),
+            pltpu.VMEM(conv_taps.shape, bf16),
+            pltpu.VMEM((layers, 2, BLOCK, cols), bf16),
+            pltpu.VMEM(decay_param.shape, f32),
+            pltpu.VMEM(w_out.shape, bf16),
+            pltpu.VMEM(prior_state.shape, f32),
+            pltpu.VMEM(window.shape, bf16),
+            pltpu.VMEM((nd, rows, own), bf16),
+            dma((5 + 7 * layers,)),
+            dma((2 * layers + 1,)),
+            dma((layers, halves, nt)),
+            dma((layers, halves, nt)),
+            dma((layers, halves, nd)),
+            dma((layers, halves, nd)),
+            dma((layers, halves, nd)),
+            dma((layers, halves, nd)),
+            dma((layers, halves, nt)),
+            dma((layers, halves, nt)),
+        ],
+        compiler_params=pltpu.CompilerParams(collective_id=0, has_side_effects=True),
+    )(
+        stream.reshape(nd, rows, own),
+        lengths.reshape(1, rows),
+        prior_state,
+        window,
+        norm_gain,
+        w_branch,
+        w_gate_branch,
+        conv_taps,
+        w_in_gate,
+        w_rec_gate,
+        decay_param,
+        w_out,
+    )
+    return mixed.reshape(batch, own), state, new_window.transpose(0, 2, 1, 3)
+
+
+def step(nt, nd, *arrays):
+    stream, w_branch = arrays[0], arrays[5]
+    rows, cols = stream.shape[0] // nd, w_branch.shape[2]
+    if cols % BLOCK == 0 and stream.shape[1] % 128 == 0 and rows % (16 * HALVES) == 0:
+        return fused(nt, nd, HALVES, *arrays)
+    return body(*arrays)
+
+
 def solution(mesh):
     placed = (
         P(None, ("dp", "tp")),
@@ -193,7 +580,7 @@
         P(None, "tp", "dp"),
     )
     return jax.shard_map(
-        body,
+        functools.partial(step, mesh.shape["tp"], mesh.shape["dp"]),
         mesh=mesh,
         in_specs=placed,
         out_specs=(P(None, ("dp", "tp")), P(None, "dp", "tp"), P(None, "dp", None, "tp")),

time: 263 us -> 53.4 us (0.20)
  blocking collectives: 129 us -> 0 us
  waiting for transfers between devices: 89.6 us -> 0 us
  Pallas kernels: 0 us -> 47.9 us
  between operations: 14.3 us -> 0.64 us
  other arithmetic: 9.79 us -> 0 us
  matrix products: 8.71 us -> 0 us
  local copies, waits for them, and re-layouts: 10.4 us -> 4.56 us
    psum x3 -> x0, blocking collectives: 91.2 us -> none  [the longest x1 43.3 us: body(): carried = lax.psum(terms, 'tp').astype(jnp.bfloat16)]
    reduce_scatter x3 -> x0, waiting for transfers between devices: 89.5 us -> none  [the longest x1 58.8 us: body(): lax.psum_scatter(terms, 'tp', scatter_dimension=1, tiled=True)]
    pallas_call x0 -> x1, Pallas kernels: none -> 47.9 us  [fused(): pl.pallas_call(functools.partial(fused_kernel, nt, nd, halves), out_shape...]
    all_gather x3 -> x0, blocking collectives: 37.4 us -> none  [the longest x1 26.4 us: normed_input(): lax.all_gather(norm_rows(stream_local, own_gain, squares), 'tp', axis=1,...]
    dot_general x10 -> x0, matrix products: 8.71 us -> none  [the longest x2 3.2 us: recurrent_step(): jnp.dot(normed, w_gate_branch, preferred_element_type=jnp.float32)]
    convert_element_type x4 -> x0, other arithmetic: 4.01 us -> none  [the longest x2 1.71 us: recurrent_step(): (state * jax.nn.gelu(gate_in.astype(jnp.float32))).astype(jnp.bfloat16)]
    div x12 -> x0, local copies, waits for them, and re-layouts: 2.97 us -> none  [recurrent_step(): input_gate = jax.nn.sigmoid(block_gates(grouped, w_in_gate))]
  transfers between devices with their start and end apart: 3 -> 0, of which waited for: 3 -> 0; matrix products, arithmetic and copies ran while one was open for 3% -> 0% of each run, Pallas kernels for 0% -> 0%
where the time goes in v1:
time: 53.4 us; the launch traced here: 53.1 us
  Pallas kernels  47.9 us (90%)
  local copies, waits for them, and re-layouts  4.56 us (9%)
  between operations  0.64 us (1%)
    pallas_call x1, Pallas kernels, fused(): pl.pallas_call(functools.partial(fused_kernel, nt, nd, halves), out_shape...  47.9 us
    unnamed x3, local copies, waits for them, and re-layouts  4.56 us

profile of v1, /device:TPU:0, one launch (start us, length us, event | category | flops | bytes accessed | tf_op | source)
XLA Modules:
  0.0 53.1 jit_solution(4356657549753986340)
XLA Ops:
  0.6 47.9 %shard_map.139 = (bf16[4,32,128]{2,1,0:T(8,128)(2,1)}, f32[2,32,512]{2,1,0:T(8,128)}, bf16[2,3,32,512]{3,2,1,0:T(8,128)(2,1)}) custom-call(bf16[4,32,128]{2,1,0:T(8,128)(2,1)} %bitcast.7, s32[1,32]{1,0:T(1,128)} %bitcast.9, f32[2,32,512]{2,1,0:T(8,128)} %prior_state.1, bf16[2,3,32,512]{3,2,1,0:T(8,128)(2,1)} %bitcast.6, f32[2,1024]{1,0:T(2,128)} %norm_gain.1, ...), custom_call_target="tpu_custom_call" | custom-call | tf_op jit(solution)/shard_map/pallas_call | solution.py:501
  48.6 1.4 %copy.18 = bf16[128,128]{1,0:T(8,128)(2,1)} copy(bf16[128,128]{1,0:T(8,128)(2,1)} %bitcast.8) | data formatting | bytes 65536
  49.9 1.6 %copy.19 = f32[2,32,512]{2,1,0:T(8,128)} copy(f32[2,32,512]{2,1,0:T(8,128)} %get-tuple-element.13) | data formatting | bytes 262144
  51.5 1.6 %copy.20 = bf16[2,32,3,512]{3,1,2,0:T(8,128)(2,1)} copy(bf16[2,32,3,512]{3,1,2,0:T(8,128)(2,1)} %bitcast.5) | data formatting | bytes 393216

commit v2 on v1

--- a/solution.py
+++ b/solution.py
@@ -181,7 +181,9 @@
     )
 
 
-HALVES = 2
+HALVES = 4
+MAIN_VMEM = 60 * 1024 * 1024
+TAIL_VMEM = 4 * 1024 * 1024
 MESH = pl.DeviceIdType.MESH
 
 
@@ -472,6 +474,21 @@
         copy.wait()
 
 
+def tail_kernel(mixed, state, window, mixed_out, state_out, window_out, a, b, c, in_sem, out_sem):
+    triples = ((mixed, a, mixed_out), (state, b, state_out), (window, c, window_out))
+    loads = []
+    for k, (src, held, _) in enumerate(triples):
+        loads.append(pltpu.make_async_copy(src, held, in_sem.at[k]))
+        loads[-1].start()
+    stores = []
+    for k, (_, held, dst) in enumerate(triples):
+        loads[k].wait()
+        stores.append(pltpu.make_async_copy(held, dst, out_sem.at[k]))
+        stores[-1].start()
+    for copy in stores:
+        copy.wait()
+
+
 def fused(
     nt,
     nd,
@@ -505,7 +522,7 @@
             jax.ShapeDtypeStruct(prior_state.shape, f32),
             jax.ShapeDtypeStruct(window.shape, bf16),
         ),
-        in_specs=[anywhere] * 12,
+        in_specs=[pl.BlockSpec(memory_space=pltpu.HBM)] * 12,
         out_specs=(anywhere,) * 3,
         scratch_shapes=[
             pltpu.VMEM((layers, nt, nd, rows, own), bf16),
@@ -538,7 +555,7 @@
             dma((layers, halves, nt)),
             dma((layers, halves, nt)),
         ],
-        compiler_params=pltpu.CompilerParams(collective_id=0, has_side_effects=True),
+        compiler_params=pltpu.CompilerParams(collective_id=0, has_side_effects=True, vmem_limit_bytes=MAIN_VMEM),
     )(
         stream.reshape(nd, rows, own),
         lengths.reshape(1, rows),
@@ -553,13 +570,22 @@
         decay_param,
         w_out,
     )
+    finals = (mixed, state, new_window)
+    mixed, state, new_window = pl.pallas_call(
+        tail_kernel,
+        out_shape=tuple(jax.ShapeDtypeStruct(a.shape, a.dtype) for a in finals),
+        in_specs=[anywhere] * 3,
+        out_specs=(anywhere,) * 3,
+        scratch_shapes=[pltpu.VMEM(a.shape, a.dtype) for a in finals] + [dma((3,)), dma((3,))],
+        compiler_params=pltpu.CompilerParams(vmem_limit_bytes=TAIL_VMEM),
+    )(*finals)
     return mixed.reshape(batch, own), state, new_window.transpose(0, 2, 1, 3)
 
 
 def step(nt, nd, *arrays):
     stream, w_branch = arrays[0], arrays[5]
     rows, cols = stream.shape[0] // nd, w_branch.shape[2]
-    if cols % BLOCK == 0 and stream.shape[1] % 128 == 0 and rows % (16 * HALVES) == 0:
+    if cols % BLOCK == 0 and stream.shape[1] % 128 == 0 and rows % (8 * HALVES) == 0:
         return fused(nt, nd, HALVES, *arrays)
     return body(*arrays)
 

time: 53.4 us -> 52.1 us (0.976)
  local copies, waits for them, and re-layouts: 4.56 us -> 2.58 us
  Pallas kernels: 47.9 us -> 48.6 us
    unnamed x3 -> x6, local copies, waits for them, and re-layouts: 4.56 us -> 2.58 us
    pallas_call x0 -> x1, Pallas kernels: none -> 1.21 us  [fused(): pl.pallas_call(tail_kernel, out_shape=tuple((jax.ShapeDtypeStruct(a.shape...]
where the time goes in v2:
time: 52.1 us; the launch traced here: 51.9 us
  Pallas kernels  48.6 us (93%)
  local copies, waits for them, and re-layouts  2.58 us (5%)
  between operations  0.65 us (1%)
    pallas_call x1, Pallas kernels, fused(): pl.pallas_call(functools.partial(fused_kernel, nt, nd, halves), out_shape...  47.4 us
    unnamed x6, local copies, waits for them, and re-layouts  2.58 us
    pallas_call x1, Pallas kernels, fused(): pl.pallas_call(tail_kernel, out_shape=tuple((jax.ShapeDtypeStruct(a.shape...  1.21 us

profile of v2, /device:TPU:0, one launch (start us, length us, event | category | flops | bytes accessed | tf_op | source)
XLA Modules:
  0.0 51.9 jit_solution(12831364921762667709)
XLA Ops:
  0.6 47.4 %shard_map.139 = (bf16[4,32,128]{2,1,0:T(8,128)(2,1)}, f32[2,32,512]{2,1,0:T(8,128)}, bf16[2,3,32,512]{3,2,1,0:T(8,128)(2,1)}) custom-call(bf16[4,32,128]{2,1,0:T(8,128)(2,1)} %bitcast.6, s32[1,32]{1,0:T(1,128)} %bitcast.7, f32[2,32,512]{2,1,0:T(8,128)} %prior_state.1, bf16[2,3,32,512]{3,2,1,0:T(8,128)(2,1)} %bitcast.5, f32[2,1024]{1,0:T(2,128)} %norm_gain.1, ...), custom_call_target="tpu_custom_call" | custom-call | tf_op jit(solution)/shard_map/pallas_call | solution.py:518
  48.1 0.0 copy-start
  48.1 0.9 %copy-done = bf16[2,3,32,512]{3,2,1,0:T(8,128)(2,1)S(1)} copy-done((bf16[2,3,32,512]{3,2,1,0:T(8,128)(2,1)S(1)}, bf16[2,3,32,512]{3,2,1,0:T(8,128)(2,1)}, u32[]{:S(2)}) %copy-start) | copy-done | bytes 196632
  49.0 0.0 copy-start.1
  49.0 0.9 %copy-done.1 = f32[2,32,512]{2,1,0:T(8,128)S(1)} copy-done((f32[2,32,512]{2,1,0:T(8,128)S(1)}, f32[2,32,512]{2,1,0:T(8,128)}, u32[]{:S(2)}) %copy-start.1) | copy-done | bytes 131096
  49.9 0.0 copy-start.2
  49.9 0.8 %copy-done.2 = bf16[4,32,128]{2,1,0:T(8,128)(2,1)S(1)} copy-done((bf16[4,32,128]{2,1,0:T(8,128)(2,1)S(1)}, bf16[4,32,128]{2,1,0:T(8,128)(2,1)}, u32[]{:S(2)}) %copy-start.2) | copy-done | bytes 32792
  50.7 1.2 %shard_map.140 = (bf16[4,32,128]{2,1,0:T(8,128)(2,1)}, f32[2,32,512]{2,1,0:T(8,128)}, bf16[2,3,32,512]{3,2,1,0:T(8,128)(2,1)}) custom-call(bf16[4,32,128]{2,1,0:T(8,128)(2,1)S(1)} %copy-done.2, f32[2,32,512]{2,1,0:T(8,128)S(1)} %copy-done.1, bf16[2,3,32,512]{3,2,1,0:T(8,128)(2,1)S(1)} %copy-done), custom_call_target="tpu_custom_call" | custom-call | tf_op jit(solution)/shard_map/pallas_call | solution.py:574
Async XLA Ops:
  48.1 0.9 %copy-start = (bf16[2,3,32,512]{3,2,1,0:T(8,128)(2,1)S(1)}, bf16[2,3,32,512]{3,2,1,0:T(8,128)(2,1)}, u32[]{:S(2)}) copy-start(bf16[2,3,32,512]{3,2,1,0:T(8,128)(2,1)} %get-tuple-element.11.window) | copy-start | bytes 589828
  49.0 0.9 %copy-start.1 = (f32[2,32,512]{2,1,0:T(8,128)S(1)}, f32[2,32,512]{2,1,0:T(8,128)}, u32[]{:S(2)}) copy-start(f32[2,32,512]{2,1,0:T(8,128)} %get-tuple-element.10.state) | copy-start | bytes 393220
  49.9 0.8 %copy-start.2 = (bf16[4,32,128]{2,1,0:T(8,128)(2,1)S(1)}, bf16[4,32,128]{2,1,0:T(8,128)(2,1)}, u32[]{:S(2)}) copy-start(bf16[4,32,128]{2,1,0:T(8,128)(2,1)} %get-tuple-element.9.mixed) | copy-start | bytes 98308
